TPU v7x, 32 devices: a whole 2x2x4 slice. The times are simulated.
32 devices in a mesh: dp: 4 (over y, x), kv: 4 (over z), tp: 2 (over core).
Axes of the slice: x: 2, y: 2, z: 4, core: 2. Of those that a mesh axis runs over, the one named last changes fastest.
Arguments:
- tokens: bfloat16 [32, 4096], P('dp', 'kv'), may hold values from -6 to 6
- token_gain: float32 [4096], P('kv'), may hold values from 0.1 to 1.9
- asker_narrow_matrix: bfloat16 [4096, 1536], P('kv'), may hold values from -0.09375 to 0.09375
- hidden_narrow_matrix: bfloat16 [4096, 1088], P('kv'), may hold values from -0.09375 to 0.09375
- asker_multiplier: float32 [1536], replicated, may hold values from 0.1 to 1.9
- hidden_multiplier: float32 [1024], replicated, may hold values from 0.1 to 1.9
- asker_unspun_matrix: bfloat16 [1536, 64, 128], P(None, ('kv', 'tp')), may hold values from -0.15625 to 0.15625
- asker_spin_matrix: bfloat16 [1536, 64, 64], P(None, ('kv', 'tp')), may hold values from -0.15625 to 0.15625
- lock_widen_matrix: bfloat16 [64, 128, 1024], P(('kv', 'tp')), may hold values from -0.25 to 0.25
- payload_widen_matrix: bfloat16 [64, 1024, 128], P(('kv', 'tp')), may hold values from -0.75 to 0.75
- w_output: bfloat16 [8192, 4096], P(('kv', 'tp')), may hold values from -0.75 to 0.75
- cache_latent: bfloat16 [32, 1024, 1024], P('dp', 'kv'), may hold values from -4 to 4
- cache_rotary: bfloat16 [32, 1024, 64], P('dp', 'kv'), may hold values from -400 to 400
- lengths: int32 [32], P('dp'), may hold values from 512 to 1023, as said below
Outputs:
- attention_out: float32 [32, 4096], P('dp', ('kv', 'tp'))
- incoming_hidden: float32 [32, 1024], P('dp')
- incoming_spun: float32 [32, 64], P('dp')
Inputs may be any that keep to these rules, and one draw needn't show every extreme that they name: `lengths`: each length lies in 512 to 1023; some sequence has 1023 and some has 512.
All inputs are finite; a program needn't handle non-finite values.
Results may differ from a plain program's by a relative error of at most 0.015.
Values may be sent and summed in bfloat16 or wider, within the bound.
A program may use at most 64 MiB of HBM per device.

v0:
```python
import jax
import jax.numpy as jnp
from jax import lax
from jax.sharding import PartitionSpec as P

MODEL_BREADTH = 4096


EPS = 1e-06
THETA = 10000.0


def magnitude_divisor(values, gain):
    mean_square = jnp.mean(values * values, axis=-1, keepdims=True)
    return values * lax.rsqrt(mean_square + EPS) * gain


def spinning(values, position):
    half_width = values.shape[-1] // 2
    exponent = jnp.arange(half_width, dtype=jnp.float32) * (2.0 / values.shape[-1])
    frequency = THETA ** (-exponent)
    angles = position.astype(jnp.float32)[:, None] * frequency[None, :]
    angles = angles.reshape((angles.shape[0],) + (1,) * (values.ndim - 2) + (half_width,))
    cosine = jnp.cos(angles)
    sine_table = jnp.sin(angles)
    former = values[..., :half_width]
    latter = values[..., half_width:]
    return jnp.concatenate(
        [former * cosine - latter * sine_table, former * sine_table + latter * cosine], axis=-1
    )


def local(
    tokens,
    token_gain,
    asker_narrow_matrix,
    hidden_narrow_matrix,
    asker_multiplier,
    hidden_multiplier,
    asker_unspun_matrix,
    asker_spin_matrix,
    lock_widen_matrix,
    payload_widen_matrix,
    w_output,
    cache_latent,
    cache_rotary,
    lengths,
):
    tokens_wide = tokens.astype(jnp.float32)
    squares = jnp.sum(tokens_wide * tokens_wide, axis=1, keepdims=True)
    scaled = (tokens_wide * token_gain).astype(jnp.bfloat16)
    query_part = jnp.dot(scaled, asker_narrow_matrix, preferred_element_type=jnp.float32)
    latent_part = jnp.dot(scaled, hidden_narrow_matrix, preferred_element_type=jnp.float32)
    squares, query_down, hidden_squeeze = lax.psum((squares, query_part, latent_part), "kv")
    row_scale = lax.rsqrt(squares / MODEL_BREADTH + EPS)
    query_down = query_down * row_scale
    hidden_squeeze = hidden_squeeze * row_scale
    seqs_here, query_width = query_down.shape
    latent_width = lock_widen_matrix.shape[2]
    own_heads = asker_unspun_matrix.shape[1]
    nope_width = asker_unspun_matrix.shape[2]
    rope_width = asker_spin_matrix.shape[2]
    value_width = payload_widen_matrix.shape[2]
    squeezed = magnitude_divisor(query_down, asker_multiplier).astype(jnp.bfloat16)
    incoming_hidden = magnitude_divisor(hidden_squeeze[:, :latent_width], hidden_multiplier)
    incoming_spun = spinning(hidden_squeeze[:, latent_width:], lengths)
    fresh_hidden = incoming_hidden.astype(jnp.bfloat16)
    fresh_spun = incoming_spun.astype(jnp.bfloat16)
    asker_unspun = jnp.dot(
        squeezed,
        asker_unspun_matrix.reshape(query_width, own_heads * nope_width),
        preferred_element_type=jnp.float32,
    )
    asker_unspun = asker_unspun.reshape(seqs_here, own_heads, nope_width).astype(jnp.bfloat16)
    query_latent = jnp.einsum(
        "shd,hdc->shc", asker_unspun, lock_widen_matrix, preferred_element_type=jnp.float32
    ).astype(jnp.bfloat16)
    asker_spun = jnp.dot(
        squeezed,
        asker_spin_matrix.reshape(query_width, own_heads * rope_width),
        preferred_element_type=jnp.float32,
    )
    asker_spun = spinning(asker_spun.reshape(seqs_here, own_heads, rope_width), lengths).astype(
        jnp.bfloat16
    )
    all_latent, all_turned = (
        lax.all_gather(query_latent, "kv", axis=1, tiled=True),
        lax.all_gather(asker_spun, "kv", axis=1, tiled=True),
    )
    span = cache_latent.shape[1]
    positions = lax.axis_index("kv") * span + jnp.arange(span, dtype=jnp.int32)
    fresh_slot = positions[None, :] == lengths[:, None]
    keys_latent = jnp.where(fresh_slot[:, :, None], fresh_hidden[:, None, :], cache_latent)
    keys_turned = jnp.where(fresh_slot[:, :, None], fresh_spun[:, None, :], cache_rotary)
    visible = (positions[None, :] <= lengths[:, None])[:, None, :]
    scores = jnp.einsum("shc,spc->shp", all_latent, keys_latent, preferred_element_type=jnp.float32)
    scores = scores + jnp.einsum(
        "shr,spr->shp", all_turned, keys_turned, preferred_element_type=jnp.float32
    )
    scores = jnp.where(visible, scores * (nope_width + rope_width) ** (-0.5), -1e30)
    local_max = jnp.max(scores, axis=2)
    weights = jnp.where(visible, jnp.exp(scores - local_max[:, :, None]), 0.0)
    local_total = jnp.sum(weights, axis=2)
    local_mix = jnp.einsum(
        "shp,spc->shc",
        weights.astype(jnp.bfloat16),
        keys_latent,
        preferred_element_type=jnp.float32,
    )
    highest = lax.pmax(local_max, "kv")
    factor = jnp.exp(local_max - highest)
    denominator, mixture = (
        lax.psum_scatter(local_total * factor, "kv", scatter_dimension=1, tiled=True),
        lax.psum_scatter(local_mix * factor[:, :, None], "kv", scatter_dimension=1, tiled=True),
    )
    attended = (mixture / denominator[:, :, None]).astype(jnp.bfloat16)
    head_values = jnp.einsum(
        "shc,hcv->shv", attended, payload_widen_matrix, preferred_element_type=jnp.float32
    ).astype(jnp.bfloat16)
    flat_values = head_values.reshape(seqs_here, own_heads * value_width)
    summed = lax.psum_scatter(
        lax.dot_general(
            w_output, flat_values, (((0,), (1,)), ((), ())), preferred_element_type=jnp.float32
        ),
        ("kv", "tp"),
        scatter_dimension=0,
        tiled=True,
    )
    return (summed.T, incoming_hidden, incoming_spun)


def solution(mesh):
    return jax.shard_map(
        local,
        mesh=mesh,
        in_specs=(
            P("dp", "kv"),
            P("kv"),
            P("kv", None),
            P("kv", None),
            P(),
            P(),
            P(None, ("kv", "tp"), None),
            P(None, ("kv", "tp"), None),
            P(("kv", "tp"), None, None),
            P(("kv", "tp"), None, None),
            P(("kv", "tp"), None),
            P("dp", "kv", None),
            P("dp", "kv", None),
            P("dp"),
        ),
        out_specs=(P("dp", ("kv", "tp")), P("dp", None), P("dp", None)),
        check_vma=False,
    )
```

profile of v0, /device:TPU:0, one launch (start us, length us, event | category | flops | bytes accessed | tf_op | source)
XLA Modules:
  0.0 176.9 jit_solution(5629276316340466822)
XLA Ops:
  7.2 0.0 copy-start
  7.2 0.0 copy-start.6
  7.2 0.0 copy-start.4
  7.2 0.0 all-reduce.4.cloned.1.call-start
  7.2 1.5 fusion.26
  8.7 3.0 %fusion.30 = f32[8,1088]{1,0:T(8,128)} fusion(bf16[1024,1088]{0,1:T(8,128)(2,1)} %param.17, bf16[8,1024]{1,0:T(8,128)(2,1)} %param.14, f32[1024]{0:T(1024)} %param.15), kind=kOutput, calls=%fused_computation.48 | convolution fusion | flops 17850368 | bytes 2283520 | tf_op jit(solution)/shard_map/dot_general | solution.py:53
  11.7 0.0 copy-done
  11.7 1.8 %fusion.32 = f32[8,1536]{1,0:T(8,128)} fusion(bf16[1024,1536]{1,0:T(8,128)(2,1)S(1)} %copy-done, bf16[8,1024]{1,0:T(8,128)(2,1)} %param.14, f32[1024]{0:T(1024)} %param.15), kind=kOutput, calls=%fused_computation.49 | convolution fusion | flops 25190400 | bytes 3215360 | tf_op jit(solution)/shard_map/dot_general | solution.py:52
  13.6 0.0 all-reduce.4.cloned.1.call-update
  13.6 0.0 reduce-scatter.4.cloned.1.call-start
  13.6 0.0 copy-done.6
  13.7 0.1 broadcast_compare_fusion.1
  13.8 37.1 %all-reduce.4.cloned.1.call-done = (f32[8,1088]{1,0:T(8,128)}, f32[8,1]{0,1:T(1,128)}, f32[8,1536]{1,0:T(8,128)}) async-done(((f32[8,1088]{1,0:T(8,128)}, f32[8,1]{0,1:T(1,128)}, f32[8,1536]{1,0:T(8,128)}), (f32[8,1088]{1,0:T(8,128)}, f32[8,1]{0,1:T(1,128)}, f32[8,1536]{1,0:T(8,128)})) %all-reduce.4.cloned.1.call-update) | async-done | bytes 84016 | tf_op jit(solution)/shard_map/psum | solution.py:54
  50.9 0.0 copy-start.2
  50.9 0.0 copy-start.3
  50.9 0.8 rsqrt_bitcast_fusion
  51.7 0.8 broadcast_multiply_fusion
  52.5 0.1 multiply_reduce_fusion.1
  52.6 1.0 multiply_reduce_fusion
  53.6 0.0 copy-done.4
  53.6 0.0 copy-start.1
  53.7 2.6 %fusion.2 = bf16[8,8,128]{2,0,1:T(8,128)(2,1)S(1)} fusion(f32[8,1536]{1,0:T(8,128)} %get-tuple-element.5, f32[1536]{0:T(1024)S(1)} %copy-done.4, f32[8]{0:T(128)S(1)} %add_rsqrt_fusion.1, f32[8]{0:T(128)S(1)} %rsqrt_bitcast_fusion, bf16[192,8,8,128]{3,2,1,0:T(8,128)(2,1)} %bitcast.50), kind=kOutput, calls=%fused_computation.5 | convolution fusion | flops 25214976 | bytes 3217472 | tf_op jit(solution)/shard_map/dot_general | solution.py:69
  56.3 0.0 copy-done.2
  56.3 0.0 copy-done.3
  56.3 0.0 copy-start.5
  56.3 0.0 copy-start.7
  56.3 0.7 fusion.7
  57.0 0.1 multiply_cosine_fusion
  57.2 0.1 subtract_convert_fusion
  57.3 0.1 pad_maximum_fusion
  57.4 13.3 %all_gather.7 = bf16[8,32,64]{2,0,1:T(8,128)(2,1)S(1)} all-gather(bf16[8,8,64]{2,0,1:T(8,128)(2,1)S(1)} %pad_maximum_fusion), channel_id=1, replica_groups=mesh['dp'=4,'kv'=4,'tp'=2] {'kv'}, dimensions={1}, use_global_device_ids=true | all-gather | bytes 40960 | tf_op jit(solution)/shard_map/all_gather | solution.py:88
  70.7 0.0 copy-done.1
  70.7 0.4 fusion.28
  71.1 0.1 copy.51
  71.2 15.7 %all_gather.6 = bf16[8,32,1024]{2,1,0:T(8,128)(2,1)S(1)} all-gather(bf16[8,8,1024]{2,1,0:T(8,128)(2,1)S(1)} %bitcast.48), channel_id=1, replica_groups=mesh['dp'=4,'kv'=4,'tp'=2] {'kv'}, dimensions={1}, use_global_device_ids=true | all-gather | bytes 655360 | tf_op jit(solution)/shard_map/all_gather | solution.py:87
  86.9 0.7 fusion.38
  87.6 0.0 copy-done.5
  87.6 0.7 fusion.39
  88.2 0.0 copy-done.7
  88.2 0.0 copy-start.8
  88.2 2.0 %fusion.1 = f32[8,32,256]{2,1,0:T(8,128)S(1)} fusion(bf16[8,32,1024]{2,1,0:T(8,128)(2,1)S(1)} %all_gather.6, bf16[8,256,1024]{2,1,0:T(8,128)(2,1)S(1)} %copy-done.7, pred[8,256]{1,0:T(8,128)(4,1)S(1)} %get-tuple-element.17, bf16[8,1024]{1,0:T(8,128)(2,1)S(1)} %get-tuple-element.10), kind=kOutput, calls=%fused_computation.3 | convolution fusion | flops 136314880 | bytes 4999168 | tf_op jit(solution)/shard_map/shc,spc->shp/dot_general | solution.py:96
  90.2 0.0 copy-done.8
  90.3 0.3 fusion.40
  90.6 11.1 %pmax.7 = f32[8,32]{1,0:T(8,128)S(1)} all-reduce(f32[8,32]{1,0:T(8,128)S(1)} %get-tuple-element.22), channel_id=1, replica_groups=mesh['dp'=4,'kv'=4,'tp'=2] {'kv'}, use_global_device_ids=true, to_apply=%region_7.8 | all-reduce | flops 256 | bytes 2048 | tf_op jit(solution)/shard_map/pmax | solution.py:110
  101.7 0.2 fusion.14
  101.9 4.2 %fusion = f32[8,32,1024]{2,1,0:T(8,128)} fusion(bf16[8,256,1024]{2,1,0:T(8,128)(2,1)} %param.25, pred[8,256]{1,0:T(8,128)(4,1)S(1)} %get-tuple-element.17, bf16[8,1024]{1,0:T(8,128)(2,1)S(1)} %get-tuple-element.10, f32[8,32,256]{2,1,0:T(8,128)S(1)} %get-tuple-element.23, f32[8,32]{1,0:T(8,128)S(1)} %get-tuple-element.22, ...), kind=kOutput, calls=%fused_computation.2 | convolution fusion | flops 136511488 | bytes 5526528 | tf_op jit(solution)/shard_map/shp,spc->shc/dot_general | solution.py:104
  106.1 0.0 copy-start.9
  106.1 0.1 copy.21
  106.1 2.9 %copy_multiply_fusion = f32[8,32,1024]{2,0,1:T(8,128)} fusion(f32[8,32,1024]{2,1,0:T(8,128)} %fusion, f32[8,32]{0,1:T(8,128)S(1)} %copy.21), kind=kLoop, calls=%fused_computation.17 | loop fusion | flops 262144 | bytes 2098176 | tf_op jit(solution)/shard_map/mul | solution.py:114
  109.0 0.0 reduce-scatter.4.cloned.1.call-update
  109.0 0.0 reduce-scatter.6.cloned.1.call-start
  109.1 0.0 copy-done.9
  109.1 0.6 dynamic-slice
  110.3 8.4 %all-reduce = f32[8,32]{1,0:T(8,128)S(1)} all-reduce(f32[8,32]{1,0:T(8,128)S(1)} %get-tuple-element.6), channel_id=3, replica_groups=mesh['dp'=4,'kv'=4,'tp'=2] {'kv'}, use_global_device_ids=true, to_apply=%region_10.11.clone | all-reduce | flops 256 | bytes 2048
  118.7 0.1 constant_dynamic-slice_fusion
  118.8 0.1 copy.22
  118.9 16.0 %reduce-scatter.4.cloned.1.call-done = f32[8,8,1024]{2,0,1:T(8,128)} async-done(((f32[8,32,1024]{2,0,1:T(8,128)}), f32[8,8,1024]{2,0,1:T(8,128)}) %reduce-scatter.4.cloned.1.call-update) | async-done | bytes 262160 | tf_op jit(solution)/shard_map/reduce_scatter | solution.py:114
  134.9 6.3 %convolution_bitcast_fusion = f32[4096,8]{0,1:T(8,128)} fusion(bf16[1024,4096]{1,0:T(8,128)(2,1)} %param.24, bf16[8,1024,128]{2,1,0:T(8,128)(2,1)} %param.23, f32[8,8,1024]{2,0,1:T(8,128)} %reduce-scatter.4.cloned.1.call-done, f32[8,8]{0,1:T(8,128)S(1)} %copy.22), kind=kOutput, calls=%fused_computation | convolution fusion | flops 84025344 | bytes 10879232 | tf_op jit(solution)/shard_map/dot_general | solution.py:122
  141.1 0.0 reduce-scatter.6.cloned.1.call-update
  141.1 29.2 %reduce-scatter.6.cloned.1.call-done = f32[512,8]{0,1:T(8,128)} async-done(((f32[4096,8]{0,1:T(8,128)}), f32[512,8]{0,1:T(8,128)}) %reduce-scatter.6.cloned.1.call-update) | async-done | bytes 16400 | tf_op jit(solution)/shard_map/reduce_scatter | solution.py:121
  (7 shorter events, 0.0 us)
Async XLA Ops:
  7.2 4.5 %copy-start = (bf16[1024,1536]{1,0:T(8,128)(2,1)S(1)}, bf16[1024,1536]{1,0:T(8,128)(2,1)}, u32[]{:S(2)}) copy-start(bf16[1024,1536]{1,0:T(8,128)(2,1)} %param.16) | copy-start | bytes 9437188
  7.2 6.5 %copy-start.6 = (s32[8]{0:T(128)S(1)}, s32[8]{0:T(128)}, u32[]{:S(2)}) copy-start(s32[8]{0:T(128)} %param.27) | copy-start | bytes 100
  7.2 46.5 %copy-start.4 = (f32[1536]{0:T(1024)S(1)}, f32[1536]{0:T(1024)}, u32[]{:S(2)}) copy-start(f32[1536]{0:T(1024)} %param.18) | copy-start | bytes 18436
  7.2 43.7 %all-reduce.4.cloned.1.call-start = ((), (), s32[]{:S(2)}) async-start(), calls=%async_computation.4 | async-start | bytes 173056 | tf_op jit(solution)/shard_map/psum | solution.py:54
  13.6 121.3 %reduce-scatter.4.cloned.1.call-start = ((), (), s32[]{:S(2)}) async-start(), calls=%async_computation.2 | async-start | bytes 1310720 | tf_op jit(solution)/shard_map/reduce_scatter | solution.py:114
  50.9 5.4 %copy-start.2 = (bf16[1536,8,64]{0,2,1:T(8,128)(2,1)S(1)}, bf16[1536,8,64]{0,2,1:T(8,128)(2,1)}, u32[]{:S(2)}) copy-start(bf16[1536,8,64]{0,2,1:T(8,128)(2,1)} %param.21) | copy-start | bytes 4718596
  50.9 5.4 %copy-start.3 = (f32[8,1536]{1,0:T(8,128)S(1)}, f32[8,1536]{1,0:T(8,128)}, u32[]{:S(2)}) copy-start(f32[8,1536]{1,0:T(8,128)} %get-tuple-element.5) | copy-start | bytes 147460
  53.6 17.0 %copy-start.1 = (bf16[8,128,1024]{2,1,0:T(8,128)(2,1)S(1)}, bf16[8,128,1024]{2,1,0:T(8,128)(2,1)}, u32[]{:S(2)}) copy-start(bf16[8,128,1024]{2,1,0:T(8,128)(2,1)} %param.22) | copy-start | bytes 6291460
  56.3 31.3 %copy-start.5 = (f32[1024]{0:T(1024)S(1)}, f32[1024]{0:T(1024)}, u32[]{:S(2)}) copy-start(f32[1024]{0:T(1024)} %param.19) | copy-start | bytes 12292
  56.3 31.9 %copy-start.7 = (bf16[8,256,1024]{2,1,0:T(8,128)(2,1)S(1)}, bf16[8,256,1024]{2,1,0:T(8,128)(2,1)}, u32[]{:S(2)}) copy-start(bf16[8,256,1024]{2,1,0:T(8,128)(2,1)} %param.25) | copy-start | bytes 12582916
  88.2 2.0 %copy-start.8 = (bf16[8,256,64]{1,2,0:T(8,128)(2,1)S(1)}, bf16[8,256,64]{1,2,0:T(8,128)(2,1)}, u32[]{:S(2)}) copy-start(bf16[8,256,64]{1,2,0:T(8,128)(2,1)} %param.26) | copy-start | bytes 786436
  106.1 3.0 %copy-start.9 = (u32[32]{0:T(128)S(1)}, u32[32]{0:T(128)}, u32[]{:S(2)}) copy-start(u32[32]{0:T(128)} %constant.33) | copy-start | bytes 388
  109.0 61.3 %reduce-scatter.6.cloned.1.call-start = ((), (), s32[]{:S(2)}) async-start(), calls=%async_computation.3 | async-start | bytes 147456 | tf_op jit(solution)/shard_map/reduce_scatter | solution.py:121
Sparse Core Ops, SparseCore 0:
  13.7 37.1 all-reduce.3
  109.1 25.6 reduce-scatter.3
  141.3 29.0 reduce-scatter.5
where the time goes:
time: 177 us
  waiting for transfers between devices  82.3 us (46%)
  blocking collectives  48.6 us (27%)
  matrix products  21.3 us (12%)
  between operations  14.6 us (8%)
  other arithmetic  9.05 us (5%)
    psum x1, waiting for transfers between devices, local(): lax.psum((squares, query_part, latent_part), 'kv')  37.1 us
    reduce_scatter x1, waiting for transfers between devices, local(): lax.psum_scatter(lax.dot_general(w_output, flat_values, (((0,), (1,)), ((...  29.2 us
    reduce_scatter x1, waiting for transfers between devices, local(): lax.psum_scatter(local_mix * factor[:, :, None], 'kv', scatter_dimension=...  16 us
    all_gather x1, blocking collectives, local(): lax.all_gather(query_latent, 'kv', axis=1, tiled=True)  15.7 us
    all_gather x1, blocking collectives, local(): lax.all_gather(asker_spun, 'kv', axis=1, tiled=True)  13.3 us
    pmax x1, blocking collectives, local(): highest = lax.pmax(local_max, 'kv')  11.1 us
    unnamed x1, blocking collectives  8.42 us
    dot_general x1, matrix products, local(): lax.dot_general(w_output, flat_values, (((0,), (1,)), ((), ())), preferre...  6.26 us
  transfers between devices with their start and end apart: 3, of which 3 were waited for; matrix products, arithmetic and copies ran while one was open for 0% of the time, Pallas kernels for 0%

commit v1 on v0

v1 whole, which is shorter than its diff:
```python
import functools

import jax
import jax.numpy as jnp
from jax import lax
from jax.experimental import pallas as pl
from jax.experimental.pallas import tpu as pltpu
from jax.sharding import PartitionSpec as P

EPS = 1e-06
THETA = 10000.0
MESH = pl.DeviceIdType.MESH
F32 = jnp.float32
BF16 = jnp.bfloat16
NT = (((1,), (1,)), ((), ()))
CHUNKS = 4


def mm(a, b):
    return jnp.dot(a, b, preferred_element_type=F32)


def mm_nt(a, b):
    return lax.dot_general(a, b, NT, preferred_element_type=F32)


def swap_halves(x, half):
    width = x.shape[1]
    if width == 2 * half:
        return jnp.concatenate([x[:, half:], x[:, :half]], axis=1)
    lane = lax.broadcasted_iota(jnp.int32, x.shape, 1)
    ahead = pltpu.roll(x, width - half, 1)
    behind = pltpu.roll(x, half, 1)
    return jnp.where((lane & (2 * half - 1)) < half, ahead, behind)


def kernel(
    dims,
    tok, gain, qmul, hmul, cos_t, sin_t, len_t,
    narrow_h, hid_h, unspun_h, spin_h, lock_h, pay_h, wout_h, lat_h, rot_h,
    out_ref, hidden_ref, spun_ref,
    narrow_q, hid_l, hid_r, unspun, spin, lock, pay, wout, lat, rot,
    ra, sa, qs, qg, mo, mr, so, sr, at, po, pr,
    load_sem,
    a_send, a_recv, t_send, t_recv, q_send, q_recv, m_send, m_recv, s_send, s_recv, o_send, o_recv,
):
    n, nt, total_width, nope_w, rope_w = dims
    me = lax.axis_index("kv")
    mt = lax.axis_index("tp")
    seqs = tok.shape[0]
    heads = lock.shape[0]
    lat_w = lock.shape[2]
    q_w = qmul.shape[1]
    qh = narrow_q.shape[1]
    lh = hid_l.shape[0]
    span = lat.shape[1]
    half = rope_w // 2
    per = seqs // CHUNKS

    loads = []

    def load(src, dst):
        copy = pltpu.make_async_copy(src, dst, load_sem.at[len(loads)])
        copy.start()
        loads.append(copy)
        return copy

    l_narrow = load(narrow_h.at[:, pl.ds(pl.multiple_of(mt * qh, 128), qh)], narrow_q)
    l_hid = load(hid_h.at[pl.ds(pl.multiple_of(mt * lh, 128), lh), :], hid_l)
    l_hr = load(hid_h.at[pl.ds(lat_w, rope_w), :], hid_r)
    l_unspun = load(unspun_h, unspun)
    l_spin = load(spin_h, spin)
    l_lock = load(lock_h, lock)
    l_lat = load(lat_h, lat)
    l_rot = load(rot_h, rot)
    l_pay = load(pay_h, pay)
    l_wout = load(wout_h, wout)

    def peer(offset):
        return lax.rem(me + offset, n)

    barrier = pltpu.get_barrier_semaphore()
    for o in range(n):
        for t in range(nt):
            if o or t:
                pl.semaphore_signal(
                    barrier, inc=1, device_id={"kv": peer(o), "tp": lax.rem(mt + t, nt)}, device_id_type=MESH
                )

    def remote(src, dst, send, recv, where):
        return pltpu.make_async_remote_copy(
            src_ref=src, dst_ref=dst, send_sem=send, recv_sem=recv, device_id=where, device_id_type=MESH
        )

    started = []

    wide = tok[...].astype(F32)
    squares = jnp.sum(wide * wide, axis=1, keepdims=True)
    scaled = (wide * gain[...]).astype(BF16)
    l_narrow.wait()
    ra[me, :, :qh] = mm(scaled, narrow_q[...])
    l_hid.wait()
    ra[me, :, qh : qh + lh] = mm_nt(scaled, hid_l[...])
    l_hr.wait()
    ra[me, :, qh + lh : qh + lh + rope_w] = mm_nt(scaled, hid_r[...])
    ra[me, :, qh + lh + rope_w :] = jnp.broadcast_to(squares, (seqs, ra.shape[2] - qh - lh - rope_w))
    pl.semaphore_wait(barrier, n * nt - 1)
    for o in range(n - 1, 0, -1):
        copy = remote(ra.at[me], ra.at[me], a_send.at[o], a_recv.at[o], {"kv": peer(o)})
        copy.start()
        started.append(copy)
    for o in range(1, n):
        src = peer(n - o)
        remote(ra.at[me], ra.at[src], a_send.at[o], a_recv.at[o], {"kv": peer(o)}).wait_recv()
    total = ra[0]
    for j in range(1, n):
        total = total + ra[j]
    sa[mt] = total[:, : qh + lh]
    for t in range(1, nt):
        for i, (lo, size) in enumerate(((0, qh), (qh, lh))):
            part = sa.at[mt, :, pl.ds(lo, size)]
            copy = remote(part, part, t_send.at[t, i], t_recv.at[t, i], {"tp": lax.rem(mt + t, nt)})
            copy.start()
            started.append(copy)
    tail = total[:, qh + lh :]
    row_scale = lax.rsqrt(tail[:, rope_w : rope_w + 1] / total_width + EPS)

    def tp_wait(i, lo, size):
        for t in range(1, nt):
            src = lax.rem(mt + nt - t, nt)
            part = sa.at[src, :, pl.ds(lo, size)]
            remote(part, part, t_send.at[t, i], t_recv.at[t, i], {"tp": lax.rem(mt + t, nt)}).wait_recv()

    tp_wait(0, 0, qh)
    query_down = jnp.concatenate([sa[t, :, :qh] for t in range(nt)], axis=1) * row_scale
    mean_square = jnp.mean(query_down * query_down, axis=1, keepdims=True)
    squeezed = (query_down * lax.rsqrt(mean_square + EPS) * qmul[...]).astype(BF16)
    squeezed_wide = squeezed.astype(F32)

    tiles = q_w // 128
    stacked = jnp.concatenate([squeezed_wide[:, j * 128 : (j + 1) * 128] for j in range(tiles)], axis=0)
    row = lax.broadcasted_iota(jnp.int32, (128, 128 * heads), 0)
    col = lax.broadcasted_iota(jnp.int32, (128, 128 * heads), 1)
    first = row * heads
    repeat = jnp.where((col >= first) & (col < first + heads), 1.0, 0.0).astype(BF16)
    spread = mm(stacked.astype(BF16), repeat)
    head_of = lax.broadcasted_iota(jnp.int32, (seqs, 128 * heads), 1) & (heads - 1)
    l_unspun.wait()
    nope = None
    for j in range(tiles):
        piece = spread[j * seqs : (j + 1) * seqs]
        left = jnp.concatenate([jnp.where(head_of == h, piece, 0.0) for h in range(heads)], axis=0)
        term = mm(left.astype(BF16), unspun[j * 128 * heads : (j + 1) * 128 * heads, :])
        nope = term if nope is None else nope + term
    l_spin.wait()
    turned = mm_nt(squeezed, spin[...])
    turned = turned * cos_t[...] + swap_halves(turned, half) * sin_t[...]
    qs[:, :, lat_w:] = jnp.zeros((seqs, heads, qs.shape[2] - lat_w), F32)
    l_lock.wait()
    for h in range(heads):
        qs[:, h, lat_w : lat_w + rope_w] = turned[:, h * rope_w : (h + 1) * rope_w]
        qs[:, h, :lat_w] = mm(nope[h * seqs : (h + 1) * seqs].astype(BF16), lock[h])
    for c in range(CHUNKS):
        for b in range(c * per, (c + 1) * per):
            qg[me, b] = qs[b].astype(BF16)
        for o in range(n - 1, 0, -1):
            part = qg.at[me, pl.ds(c * per, per)]
            copy = remote(part, part, q_send.at[o, c], q_recv.at[o, c], {"kv": peer(o)})
            copy.start()
            started.append(copy)

    tp_wait(1, qh, lh)
    hid = jnp.concatenate([sa[t, :, qh:] for t in range(nt)], axis=1) * row_scale
    hid_square = jnp.mean(hid * hid, axis=1, keepdims=True)
    incoming = hid * lax.rsqrt(hid_square + EPS) * hmul[...]
    hidden_ref[...] = incoming
    fresh = incoming.astype(BF16).astype(F32)
    tail = tail * row_scale
    spun = tail[:, :rope_w] * cos_t[:, :rope_w] + swap_halves(tail, half)[:, :rope_w] * sin_t[:, :rope_w]
    spun_ref[...] = spun
    fresh_spun = spun.astype(BF16).astype(F32)

    all_heads = n * heads
    position = me * span + lax.broadcasted_iota(jnp.int32, (1, span), 1)
    lane = lax.broadcasted_iota(jnp.int32, (all_heads, 128), 1)
    stats = jnp.zeros((all_heads, 128), F32)
    scale = (nope_w + rope_w) ** (-0.5)
    l_lat.wait()
    l_rot.wait()
    for c in range(CHUNKS):
        for o in range(1, n):
            part = qg.at[peer(n - o), pl.ds(c * per, per)]
            remote(part, part, q_send.at[o, c], q_recv.at[o, c], {"kv": peer(o)}).wait_recv()
        for b in range(c * per, (c + 1) * per):
            query = jnp.concatenate([qg[j, b].astype(F32) for j in range(n)], axis=0)
            q_lat = query[:, :lat_w]
            q_rot = query[:, lat_w : lat_w + rope_w]
            keys = lat[b]
            length = len_t[b : b + 1, :]
            is_fresh = position == length
            visible = position <= length
            scores = mm_nt(q_lat.astype(BF16), keys) + mm(q_rot.astype(BF16), rot[b])
            fresh_score = jnp.sum(q_lat * fresh[b : b + 1, :], axis=1, keepdims=True) + jnp.sum(
                q_rot * fresh_spun[b : b + 1, :], axis=1, keepdims=True
            )
            scores = jnp.where(is_fresh, fresh_score, scores) * scale
            scores = jnp.where(visible, scores, -1e30)
            top = jnp.max(scores, axis=1, keepdims=True)
            weights = jnp.where(visible, jnp.exp(scores - top), 0.0)
            mass = jnp.sum(weights, axis=1, keepdims=True)
            rounded = weights.astype(BF16).astype(F32)
            fresh_weight = jnp.sum(jnp.where(is_fresh, rounded, 0.0), axis=1, keepdims=True)
            rounded = jnp.where(is_fresh, 0.0, rounded).astype(BF16)
            mix = mm(rounded, keys) + fresh_weight * fresh[b : b + 1, :]
            stats = jnp.where(lane == b, top, stats)
            stats = jnp.where(lane == seqs + b, mass, stats)
            for j in range(n):
                mo[j, b] = mix[j * heads : (j + 1) * heads].astype(BF16)
        for o in range(n - 1, 0, -1):
            to = peer(o)
            rows = pl.ds(c * per, per)
            copy = remote(mo.at[to, rows], mr.at[me, rows], m_send.at[o, c], m_recv.at[o, c], {"kv": to})
            copy.start()
            started.append(copy)
        if c == CHUNKS - 1:
            for j in range(n):
                so[j] = stats[j * heads : (j + 1) * heads]
            for o in range(n - 1, 0, -1):
                to = peer(o)
                copy = remote(so.at[to], sr.at[me], s_send.at[o], s_recv.at[o], {"kv": to})
                copy.start()
                started.append(copy)
    sr[me] = so[me]
    for b in range(seqs):
        mr[me, b] = mo[me, b]
    for o in range(1, n):
        src = peer(n - o)
        remote(so.at[src], sr.at[src], s_send.at[o], s_recv.at[o], {"kv": peer(o)}).wait_recv()
    all_stats = [sr[j] for j in range(n)]
    highest = all_stats[0]
    for s in all_stats[1:]:
        highest = jnp.maximum(highest, s)
    factors = [jnp.exp(jnp.minimum(s - highest, 0.0)) for s in all_stats]
    for c in range(CHUNKS):
        for o in range(1, n):
            src = peer(n - o)
            rows = pl.ds(c * per, per)
            remote(mo.at[src, rows], mr.at[src, rows], m_send.at[o, c], m_recv.at[o, c], {"kv": peer(o)}).wait_recv()
        for b in range(c * per, (c + 1) * per):
            mixture = None
            for j in range(n):
                f = factors[j][:, b : b + 1]
                term = mr[j, b].astype(F32) * f
                mass = all_stats[j][:, seqs + b : seqs + b + 1] * f
                mixture = term if mixture is None else mixture + term
                denominator = mass if j == 0 else denominator + mass
            at[b] = mixture / denominator

    l_pay.wait()
    values = jnp.concatenate([mm(at[:, h, :].astype(BF16), pay[h]) for h in range(heads)], axis=1).astype(BF16)
    l_wout.wait()
    block = out_ref.shape[1]
    mine = me * nt + mt
    for k in range(n * nt):
        po[k] = mm(values, wout[:, k * block : (k + 1) * block]).astype(BF16)

        @pl.when(mine != k)
        def _():
            remote(
                po.at[k], pr.at[mine], o_send.at[k], o_recv.at[mine], {"kv": k // nt, "tp": k % nt}
            ).start()

    pr[mine] = po[mine]
    for k in range(n * nt):

        @pl.when(mine != k)
        def _():
            remote(
                po.at[k], pr.at[k], o_send.at[k], o_recv.at[k], {"kv": k // nt, "tp": k % nt}
            ).wait()

    summed = pr[0].astype(F32)
    for k in range(1, n * nt):
        summed = summed + pr[k].astype(F32)
    out_ref[...] = summed
    for copy in started:
        copy.wait_send()


def local(
    n, nt,
    tokens, token_gain, asker_narrow_matrix, hidden_narrow_matrix, asker_multiplier, hidden_multiplier,
    asker_unspun_matrix, asker_spin_matrix, lock_widen_matrix, payload_widen_matrix, w_output,
    cache_latent, cache_rotary, lengths,
):
    seqs, width = tokens.shape
    q_w, heads, nope_w = asker_unspun_matrix.shape
    rope_w = asker_spin_matrix.shape[2]
    lat_w = lock_widen_matrix.shape[2]
    span = cache_latent.shape[1]
    model = w_output.shape[1]
    block = model // (n * nt)
    exponent = jnp.arange(rope_w // 2, dtype=F32) * (2.0 / rope_w)
    frequency = THETA ** (-exponent)
    sign = jnp.tile(jnp.repeat(jnp.array([-1.0, 1.0], F32), rope_w // 2), heads)
    angles = lengths.astype(F32)[:, None] * jnp.tile(frequency, 2 * heads)[None, :]
    cos_t = jnp.cos(angles)
    sin_t = jnp.sin(angles) * sign[None, :]
    len_t = jnp.broadcast_to(lengths[:, None], (seqs, span))
    qh, lh = q_w // nt, lat_w // nt
    tail = max(128, 2 * rope_w)
    qs_w = lat_w + max(128, rope_w)
    vm = pl.BlockSpec(memory_space=pltpu.VMEM)
    hbm = pl.BlockSpec(memory_space=pl.ANY)
    dma = pltpu.SemaphoreType.DMA
    operands = (
        tokens, token_gain[None, :], asker_multiplier[None, :], hidden_multiplier[None, :], cos_t, sin_t, len_t,
        asker_narrow_matrix,
        hidden_narrow_matrix.T,
        asker_unspun_matrix.reshape(q_w * heads, nope_w),
        asker_spin_matrix.transpose(1, 2, 0).reshape(heads * rope_w, q_w),
        lock_widen_matrix, payload_widen_matrix, w_output, cache_latent,
        cache_rotary.transpose(0, 2, 1),
    )
    scratch = [
        pltpu.VMEM((width, qh), BF16),
        pltpu.VMEM((lh, width), BF16),
        pltpu.VMEM((rope_w, width), BF16),
        pltpu.VMEM((q_w * heads, nope_w), BF16),
        pltpu.VMEM((heads * rope_w, q_w), BF16),
        pltpu.VMEM(lock_widen_matrix.shape, BF16),
        pltpu.VMEM(payload_widen_matrix.shape, BF16),
        pltpu.VMEM(w_output.shape, BF16),
        pltpu.VMEM(cache_latent.shape, BF16),
        pltpu.VMEM((seqs, rope_w, span), BF16),
        pltpu.VMEM((n, seqs, qh + lh + tail), F32),
        pltpu.VMEM((nt, seqs, qh + lh), F32),
        pltpu.VMEM((seqs, heads, qs_w), F32),
        pltpu.VMEM((n, seqs, heads, qs_w), BF16),
        pltpu.VMEM((n, seqs, heads, lat_w), BF16),
        pltpu.VMEM((n, seqs, heads, lat_w), BF16),
        pltpu.VMEM((n, heads, 128), F32),
        pltpu.VMEM((n, heads, 128), F32),
        pltpu.VMEM((seqs, heads, lat_w), F32),
        pltpu.VMEM((n * nt, seqs, block), BF16),
        pltpu.VMEM((n * nt, seqs, block), BF16),
        dma((10,)),
        dma((n,)), dma((n,)),
        dma((nt, 2)), dma((nt, 2)),
        dma((n, CHUNKS)), dma((n, CHUNKS)),
        dma((n, CHUNKS)), dma((n, CHUNKS)),
        dma((n,)), dma((n,)),
        dma((n * nt,)), dma((n * nt,)),
    ]
    return pl.pallas_call(
        functools.partial(kernel, (n, nt, width * n, nope_w, rope_w)),
        out_shape=(
            jax.ShapeDtypeStruct((seqs, block), F32),
            jax.ShapeDtypeStruct((seqs, lat_w), F32),
            jax.ShapeDtypeStruct((seqs, rope_w), F32),
        ),
        in_specs=[vm] * 7 + [hbm] * 9,
        out_specs=(vm, vm, vm),
        scratch_shapes=scratch,
        compiler_params=pltpu.CompilerParams(
            collective_id=0, has_side_effects=True, vmem_limit_bytes=60 * 1024 * 1024
        ),
    )(*operands)


def solution(mesh):
    return jax.shard_map(
        functools.partial(local, mesh.shape["kv"], mesh.shape["tp"]),
        mesh=mesh,
        in_specs=(
            P("dp", "kv"),
            P("kv"),
            P("kv", None),
            P("kv", None),
            P(),
            P(),
            P(None, ("kv", "tp"), None),
            P(None, ("kv", "tp"), None),
            P(("kv", "tp"), None, None),
            P(("kv", "tp"), None, None),
            P(("kv", "tp"), None),
            P("dp", "kv", None),
            P("dp", "kv", None),
            P("dp"),
        ),
        out_specs=(P("dp", ("kv", "tp")), P("dp", None), P("dp", None)),
        check_vma=False,
    )
```

time: 177 us -> 56.3 us (0.32)
  waiting for transfers between devices: 82.3 us -> 0 us
  blocking collectives: 48.6 us -> 0 us
  Pallas kernels: 0 us -> 46.2 us
  matrix products: 21.3 us -> 0 us
  between operations: 14.6 us -> 0.64 us
  other arithmetic: 9.05 us -> 1.43 us
  local copies, waits for them, and re-layouts: 0.96 us -> 7.56 us
    pallas_call x0 -> x1, Pallas kernels: none -> 46.2 us  [local(): pl.pallas_call(functools.partial(kernel, (n, nt, width * n, nope_w, rope_...]
    reduce_scatter x2 -> x0, waiting for transfers between devices: 45.2 us -> none  [the longest x1 29.2 us: local(): lax.psum_scatter(lax.dot_general(w_output, flat_values, (((0,), (1,)), ((...]
    psum x1 -> x0, waiting for transfers between devices: 37.1 us -> none  [local(): lax.psum((squares, query_part, latent_part), 'kv')]
    all_gather x2 -> x0, blocking collectives: 29.1 us -> none  [the longest x1 15.7 us: local(): lax.all_gather(query_latent, 'kv', axis=1, tiled=True)]
    dot_general x9 -> x0, matrix products: 21.3 us -> none  [the longest x1 6.26 us: local(): lax.dot_general(w_output, flat_values, (((0,), (1,)), ((), ())), preferre...]
    pmax x1 -> x0, blocking collectives: 11.1 us -> none  [local(): highest = lax.pmax(local_max, 'kv')]
    unnamed x1 -> x0, blocking collectives: 8.42 us -> none
    mul x4 -> x1, other arithmetic: 4.49 us -> 0.76 us  [local(): sin_t = jnp.sin(angles) * sign[None, :]]
  transfers between devices with their start and end apart: 3 -> 0, of which waited for: 3 -> 0; matrix products, arithmetic and copies ran while one was open for 0% -> 0% of each run, Pallas kernels for 0% -> 0%
where the time goes in v1:
time: 56.3 us; the launch traced here: 55.8 us
  Pallas kernels  46.2 us (82%)
  local copies, waits for them, and re-layouts  7.56 us (13%)
  other arithmetic  1.43 us (3%)
  between operations  0.64 us (1%)
    pallas_call x1, Pallas kernels, local(): pl.pallas_call(functools.partial(kernel, (n, nt, width * n, nope_w, rope_...  46.2 us
    unnamed x3, local copies, waits for them, and re-layouts  3.97 us
    broadcast_in_dim x1, local copies, waits for them, and re-layouts, local(): len_t = jnp.broadcast_to(lengths[:, None], (seqs, span))  1.32 us
    broadcast_in_dim x1, local copies, waits for them, and re-layouts, local(): asker_multiplier[None, :]  1.3 us

profile of v1, /device:TPU:0, one launch (start us, length us, event | category | flops | bytes accessed | tf_op | source)
XLA Modules:
  0.0 55.8 jit_solution(13959359301690729563)
XLA Ops:
  0.6 0.7 %convert_element_type.3 = f32[8]{0:T(128)S(1)} convert(s32[8]{0:T(128)} %param.28) | non-fusion elementwise | flops 8 | bytes 64 | tf_op jit(solution)/shard_map/convert_element_type | solution.py:306
  1.3 0.7 %broadcast_in_dim.22 = f32[2,32]{1,0:T(2,128)S(1)} broadcast(f32[2]{0:T(128)} %constant.6.clone), dimensions={0} | broadcast | bytes 264 | tf_op jit(solution)/shard_map/broadcast_in_dim | solution.py:305
  2.0 0.1 tile.14
  2.1 0.1 mul.41
  2.2 1.3 %broadcast_in_dim.20.qmul = f32[1,1536]{1,0:T(1,128)} reshape(f32[1536]{0:T(1024)} %param.19) | data formatting | bytes 12288 | tf_op jit(solution)/shard_map/broadcast_in_dim | solution.py:317
  3.5 0.1 mul.38
  3.6 1.3 %broadcast_in_dim.23.len_t = s32[8,256]{1,0:T(8,128)} broadcast(s32[8]{0:T(128)} %param.28), dimensions={0} | broadcast | bytes 8224 | tf_op jit(solution)/shard_map/broadcast_in_dim | solution.py:309
  4.9 0.8 %fusion = (f32[8,512]{1,0:T(8,128)}, f32[8,512]{1,0:T(8,128)}) fusion(f32[512]{0:T(512)S(1)} %mul.41, f32[512]{0:T(512)S(1)} %mul.38, f32[8]{0:T(128)S(1)} %convert_element_type.3), kind=kLoop, calls=%fused_computation.2 | loop fusion | flops 8192 | bytes 36896 | tf_op jit(solution)/shard_map/mul | solution.py:308
  5.7 46.2 %shard_map.166 = (f32[8,512]{1,0:T(8,128)}, f32[8,1024]{1,0:T(8,128)}, f32[8,64]{1,0:T(8,128)}) custom-call(bf16[8,1024]{1,0:T(8,128)(2,1)} %tok.1, f32[1,1024]{1,0:T(1,128)} %bitcast.12, f32[1,1536]{1,0:T(1,128)} %broadcast_in_dim.20.qmul, f32[1,1024]{1,0:T(1,128)} %bitcast.13, f32[8,512]{1,0:T(8,128)} %get-tuple-element.4.cos_t, ...), custom_call_target="tpu_custom_call" | custom-call | tf_op jit(solution)/shard_map/pallas_call | solution.py:355
  51.9 1.3 %copy.21 = f32[8,512]{1,0:T(8,128)} copy(f32[8,512]{1,0:T(8,128)} %get-tuple-element.8) | data formatting | bytes 32768
  53.2 1.4 %copy.22 = f32[8,1024]{1,0:T(8,128)} copy(f32[8,1024]{1,0:T(8,128)} %get-tuple-element.9) | data formatting | bytes 65536
  54.6 1.3 %copy.23 = f32[8,64]{1,0:T(8,128)} copy(f32[8,64]{1,0:T(8,128)} %get-tuple-element.10) | data formatting | bytes 4096
  (3 shorter events, 0.0 us)

commit v2 on v1

--- a/solution.py
+++ b/solution.py
@@ -2,6 +2,7 @@
 
 import jax
 import jax.numpy as jnp
+import numpy as np
 from jax import lax
 from jax.experimental import pallas as pl
 from jax.experimental.pallas import tpu as pltpu
@@ -36,13 +37,13 @@
 
 def kernel(
     dims,
-    tok, gain, qmul, hmul, cos_t, sin_t, len_t,
+    lens, tok, gain, qmul_t, hmul, freq,
     narrow_h, hid_h, unspun_h, spin_h, lock_h, pay_h, wout_h, lat_h, rot_h,
     out_ref, hidden_ref, spun_ref,
     narrow_q, hid_l, hid_r, unspun, spin, lock, pay, wout, lat, rot,
-    ra, sa, qs, qg, mo, mr, so, sr, at, po, pr,
+    ra, rh, sa, qs, qg, mo, mr, so, sr, at, po, pr,
     load_sem,
-    a_send, a_recv, t_send, t_recv, q_send, q_recv, m_send, m_recv, s_send, s_recv, o_send, o_recv,
+    a_send, a_recv, h_send, h_recv, t_send, t_recv, q_send, q_recv, m_send, m_recv, s_send, s_recv, o_send, o_recv,
 ):
     n, nt, total_width, nope_w, rope_w = dims
     me = lax.axis_index("kv")
@@ -50,7 +51,7 @@
     seqs = tok.shape[0]
     heads = lock.shape[0]
     lat_w = lock.shape[2]
-    q_w = qmul.shape[1]
+    q_w = qmul_t.shape[0] * qmul_t.shape[1]
     qh = narrow_q.shape[1]
     lh = hid_l.shape[0]
     span = lat.shape[1]
@@ -68,14 +69,6 @@
     l_narrow = load(narrow_h.at[:, pl.ds(pl.multiple_of(mt * qh, 128), qh)], narrow_q)
     l_hid = load(hid_h.at[pl.ds(pl.multiple_of(mt * lh, 128), lh), :], hid_l)
     l_hr = load(hid_h.at[pl.ds(lat_w, rope_w), :], hid_r)
-    l_unspun = load(unspun_h, unspun)
-    l_spin = load(spin_h, spin)
-    l_lock = load(lock_h, lock)
-    l_lat = load(lat_h, lat)
-    l_rot = load(rot_h, rot)
-    l_pay = load(pay_h, pay)
-    l_wout = load(wout_h, wout)
-
     def peer(offset):
         return lax.rem(me + offset, n)
 
@@ -94,35 +87,60 @@
 
     started = []
 
+    seq_row = lax.broadcasted_iota(jnp.int32, (seqs, 1), 0)
+    length_col = jnp.zeros((seqs, 1), jnp.int32)
+    for b in range(seqs):
+        length_col = jnp.where(seq_row == b, lens[b], length_col)
+    angles = length_col.astype(F32) * freq[...]
+    cos_t = jnp.cos(angles)
+    sin_t = jnp.sin(angles)
+    in_former = (lax.broadcasted_iota(jnp.int32, angles.shape, 1) & (rope_w - 1)) < half
+    sin_t = jnp.where(in_former, -sin_t, sin_t)
+    qmul = jnp.concatenate([qmul_t[j : j + 1, :] for j in range(qmul_t.shape[0])], axis=1)
+
     wide = tok[...].astype(F32)
     squares = jnp.sum(wide * wide, axis=1, keepdims=True)
     scaled = (wide * gain[...]).astype(BF16)
     l_narrow.wait()
+    l_hr.wait()
     ra[me, :, :qh] = mm(scaled, narrow_q[...])
-    l_hid.wait()
-    ra[me, :, qh : qh + lh] = mm_nt(scaled, hid_l[...])
-    l_hr.wait()
-    ra[me, :, qh + lh : qh + lh + rope_w] = mm_nt(scaled, hid_r[...])
-    ra[me, :, qh + lh + rope_w :] = jnp.broadcast_to(squares, (seqs, ra.shape[2] - qh - lh - rope_w))
+    ra[me, :, qh : qh + rope_w] = mm_nt(scaled, hid_r[...])
+    ra[me, :, qh + rope_w :] = jnp.broadcast_to(squares, (seqs, ra.shape[2] - qh - rope_w))
     pl.semaphore_wait(barrier, n * nt - 1)
     for o in range(n - 1, 0, -1):
         copy = remote(ra.at[me], ra.at[me], a_send.at[o], a_recv.at[o], {"kv": peer(o)})
         copy.start()
         started.append(copy)
+    l_hid.wait()
+    l_unspun = load(unspun_h, unspun)
+    l_spin = load(spin_h, spin)
+    l_lock = load(lock_h, lock)
+    rh[me] = mm_nt(scaled, hid_l[...])
+    for o in range(n - 1, 0, -1):
+        copy = remote(rh.at[me], rh.at[me], h_send.at[o], h_recv.at[o], {"kv": peer(o)})
+        copy.start()
+        started.append(copy)
+
+    def tp_send(i, lo, size):
+        part = sa.at[mt, :, pl.ds(lo, size)]
+        for t in range(1, nt):
+            copy = remote(part, part, t_send.at[t, i], t_recv.at[t, i], {"tp": lax.rem(mt + t, nt)})
+            copy.start()
+            started.append(copy)
+
     for o in range(1, n):
         src = peer(n - o)
         remote(ra.at[me], ra.at[src], a_send.at[o], a_recv.at[o], {"kv": peer(o)}).wait_recv()
     total = ra[0]
     for j in range(1, n):
         total = total + ra[j]
-    sa[mt] = total[:, : qh + lh]
-    for t in range(1, nt):
-        for i, (lo, size) in enumerate(((0, qh), (qh, lh))):
-            part = sa.at[mt, :, pl.ds(lo, size)]
-            copy = remote(part, part, t_send.at[t, i], t_recv.at[t, i], {"tp": lax.rem(mt + t, nt)})
-            copy.start()
-            started.append(copy)
-    tail = total[:, qh + lh :]
+    sa[mt, :, :qh] = total[:, :qh]
+    tp_send(0, 0, qh)
+    l_lat = load(lat_h, lat)
+    l_rot = load(rot_h, rot)
+    l_pay = load(pay_h, pay)
+    l_wout = load(wout_h, wout)
+    tail = total[:, qh:]
     row_scale = lax.rsqrt(tail[:, rope_w : rope_w + 1] / total_width + EPS)
 
     def tp_wait(i, lo, size):
@@ -134,7 +152,7 @@
     tp_wait(0, 0, qh)
     query_down = jnp.concatenate([sa[t, :, :qh] for t in range(nt)], axis=1) * row_scale
     mean_square = jnp.mean(query_down * query_down, axis=1, keepdims=True)
-    squeezed = (query_down * lax.rsqrt(mean_square + EPS) * qmul[...]).astype(BF16)
+    squeezed = (query_down * lax.rsqrt(mean_square + EPS) * qmul).astype(BF16)
     squeezed_wide = squeezed.astype(F32)
 
     tiles = q_w // 128
@@ -154,7 +172,7 @@
         nope = term if nope is None else nope + term
     l_spin.wait()
     turned = mm_nt(squeezed, spin[...])
-    turned = turned * cos_t[...] + swap_halves(turned, half) * sin_t[...]
+    turned = turned * cos_t + swap_halves(turned, half) * sin_t
     qs[:, :, lat_w:] = jnp.zeros((seqs, heads, qs.shape[2] - lat_w), F32)
     l_lock.wait()
     for h in range(heads):
@@ -169,6 +187,14 @@
             copy.start()
             started.append(copy)
 
+    for o in range(1, n):
+        src = peer(n - o)
+        remote(rh.at[me], rh.at[src], h_send.at[o], h_recv.at[o], {"kv": peer(o)}).wait_recv()
+    total = rh[0]
+    for j in range(1, n):
+        total = total + rh[j]
+    sa[mt, :, qh:] = total
+    tp_send(1, qh, lh)
     tp_wait(1, qh, lh)
     hid = jnp.concatenate([sa[t, :, qh:] for t in range(nt)], axis=1) * row_scale
     hid_square = jnp.mean(hid * hid, axis=1, keepdims=True)
@@ -196,7 +222,7 @@
             q_lat = query[:, :lat_w]
             q_rot = query[:, lat_w : lat_w + rope_w]
             keys = lat[b]
-            length = len_t[b : b + 1, :]
+            length = lens[b]
             is_fresh = position == length
             visible = position <= length
             scores = mm_nt(q_lat.astype(BF16), keys) + mm(q_rot.astype(BF16), rot[b])
@@ -287,6 +313,11 @@
         copy.wait_send()
 
 
+def hand_on(*refs):
+    for source, target in zip(refs[:3], refs[3:]):
+        target[...] = source[...]
+
+
 def local(
     n, nt,
     tokens, token_gain, asker_narrow_matrix, hidden_narrow_matrix, asker_multiplier, hidden_multiplier,
@@ -300,13 +331,8 @@
     span = cache_latent.shape[1]
     model = w_output.shape[1]
     block = model // (n * nt)
-    exponent = jnp.arange(rope_w // 2, dtype=F32) * (2.0 / rope_w)
-    frequency = THETA ** (-exponent)
-    sign = jnp.tile(jnp.repeat(jnp.array([-1.0, 1.0], F32), rope_w // 2), heads)
-    angles = lengths.astype(F32)[:, None] * jnp.tile(frequency, 2 * heads)[None, :]
-    cos_t = jnp.cos(angles)
-    sin_t = jnp.sin(angles) * sign[None, :]
-    len_t = jnp.broadcast_to(lengths[:, None], (seqs, span))
+    frequency = THETA ** (-np.arange(rope_w // 2) * (2.0 / rope_w))
+    freq = np.tile(frequency, 2 * heads)[None, :].astype(np.float32)
     qh, lh = q_w // nt, lat_w // nt
     tail = max(128, 2 * rope_w)
     qs_w = lat_w + max(128, rope_w)
@@ -314,7 +340,7 @@
     hbm = pl.BlockSpec(memory_space=pl.ANY)
     dma = pltpu.SemaphoreType.DMA
     operands = (
-        tokens, token_gain[None, :], asker_multiplier[None, :], hidden_multiplier[None, :], cos_t, sin_t, len_t,
+        lengths, tokens, token_gain[None, :], asker_multiplier.reshape(-1, 128), hidden_multiplier[None, :], freq,
         asker_narrow_matrix,
         hidden_narrow_matrix.T,
         asker_unspun_matrix.reshape(q_w * heads, nope_w),
@@ -333,7 +359,8 @@
         pltpu.VMEM(w_output.shape, BF16),
         pltpu.VMEM(cache_latent.shape, BF16),
         pltpu.VMEM((seqs, rope_w, span), BF16),
-        pltpu.VMEM((n, seqs, qh + lh + tail), F32),
+        pltpu.VMEM((n, seqs, qh + tail), F32),
+        pltpu.VMEM((n, seqs, lh), F32),
         pltpu.VMEM((nt, seqs, qh + lh), F32),
         pltpu.VMEM((seqs, heads, qs_w), F32),
         pltpu.VMEM((n, seqs, heads, qs_w), BF16),
@@ -346,26 +373,33 @@
         pltpu.VMEM((n * nt, seqs, block), BF16),
         dma((10,)),
         dma((n,)), dma((n,)),
+        dma((n,)), dma((n,)),
         dma((nt, 2)), dma((nt, 2)),
         dma((n, CHUNKS)), dma((n, CHUNKS)),
         dma((n, CHUNKS)), dma((n, CHUNKS)),
         dma((n,)), dma((n,)),
         dma((n * nt,)), dma((n * nt,)),
     ]
-    return pl.pallas_call(
+    results = pl.pallas_call(
         functools.partial(kernel, (n, nt, width * n, nope_w, rope_w)),
         out_shape=(
             jax.ShapeDtypeStruct((seqs, block), F32),
             jax.ShapeDtypeStruct((seqs, lat_w), F32),
             jax.ShapeDtypeStruct((seqs, rope_w), F32),
         ),
-        in_specs=[vm] * 7 + [hbm] * 9,
+        in_specs=[pl.BlockSpec(memory_space=pltpu.SMEM)] + [vm] * 5 + [hbm] * 9,
         out_specs=(vm, vm, vm),
         scratch_shapes=scratch,
         compiler_params=pltpu.CompilerParams(
             collective_id=0, has_side_effects=True, vmem_limit_bytes=60 * 1024 * 1024
         ),
     )(*operands)
+    return pl.pallas_call(
+        hand_on,
+        out_shape=tuple(jax.ShapeDtypeStruct(x.shape, x.dtype) for x in results),
+        in_specs=[vm] * 3,
+        out_specs=(vm, vm, vm),
+    )(*results)
 
 
 def solution(mesh):

time: 56.3 us -> 47.9 us (0.85)
  local copies, waits for them, and re-layouts: 7.56 us -> 0 us
  other arithmetic: 1.43 us -> 0 us
  Pallas kernels: 46.2 us -> 47 us
    unnamed x3 -> x0, local copies, waits for them, and re-layouts: 3.97 us -> none
    broadcast_in_dim x3 -> x0, local copies, waits for them, and re-layouts: 3.34 us -> none  [the longest x1 1.32 us: local(): len_t = jnp.broadcast_to(lengths[:, None], (seqs, span))]
    pallas_call x0 -> x1, Pallas kernels: none -> 1.38 us  [local(): pl.pallas_call(hand_on, out_shape=tuple((jax.ShapeDtypeStruct(x.shape, x....]
    mul x1 -> x0, other arithmetic: 0.76 us -> none  [local(): sin_t = jnp.sin(angles) * sign[None, :]]
    convert_element_type x1 -> x0, other arithmetic: 0.66 us -> none  [local(): lengths.astype(F32)[:, None] * jnp.tile(frequency, 2 * heads)[None, :]]
where the time goes in v2:
time: 47.9 us; the launch traced here: 47.7 us
  Pallas kernels  47 us (98%)
  between operations  0.64 us (1%)
    pallas_call x1, Pallas kernels, local(): pl.pallas_call(functools.partial(kernel, (n, nt, width * n, nope_w, rope_...  45.6 us
    pallas_call x1, Pallas kernels, local(): pl.pallas_call(hand_on, out_shape=tuple((jax.ShapeDtypeStruct(x.shape, x....  1.38 us

profile of v2, /device:TPU:0, one launch (start us, length us, event | category | flops | bytes accessed | tf_op | source)
XLA Modules:
  0.0 47.7 jit_solution(4594243013505548759)
XLA Ops:
  0.6 45.6 %shard_map.166 = (f32[8,512]{1,0:T(8,128)}, f32[8,1024]{1,0:T(8,128)}, f32[8,64]{1,0:T(8,128)}) custom-call(s32[8]{0:T(128)} %lens.1, bf16[8,1024]{1,0:T(8,128)(2,1)} %tok.1, f32[1,1024]{1,0:T(1,128)} %bitcast.14, f32[12,128]{1,0:T(8,128)} %bitcast.13, f32[1,1024]{1,0:T(1,128)} %bitcast.15, f32[1,512]{1,0:T(1,128)} %constant.2.clone.freq, ...), custom_call_target="tpu_custom_call" | custom-call | tf_op jit(solution)/shard_map/pallas_call | solution.py:383
  46.3 1.4 %shard_map.167 = (f32[8,512]{1,0:T(8,128)}, f32[8,1024]{1,0:T(8,128)}, f32[8,64]{1,0:T(8,128)}) custom-call(f32[8,512]{1,0:T(8,128)} %get-tuple-element.6.refs_0_, f32[8,1024]{1,0:T(8,128)} %get-tuple-element.7.refs_1_, f32[8,64]{1,0:T(8,128)} %get-tuple-element.8.refs_2_), custom_call_target="tpu_custom_call" | custom-call | tf_op jit(solution)/shard_map/pallas_call | solution.py:397

commit v3 on v2

--- a/solution.py
+++ b/solution.py
@@ -154,6 +154,35 @@
     mean_square = jnp.mean(query_down * query_down, axis=1, keepdims=True)
     squeezed = (query_down * lax.rsqrt(mean_square + EPS) * qmul).astype(BF16)
     squeezed_wide = squeezed.astype(F32)
+
+    bits = [1 << i for i in reversed(range(n.bit_length() - 1))]
+
+    def across(offset):
+        index = me
+        for bit in bits:
+            if offset & bit:
+                index = index + bit - 2 * bit * lax.rem(index // bit, 2)
+        return index
+
+    def query_copy(held, bit, c):
+        part = qg.at[across(held), pl.ds(c * per, per)]
+        copy = remote(part, part, q_send.at[held ^ bit, c], q_recv.at[held ^ bit, c], {"kv": across(bit)})
+        started.append(copy)
+        return copy
+
+    def query_wait(offset, bit, c):
+        part = qg.at[across(offset), pl.ds(c * per, per)]
+        remote(part, part, q_send.at[offset, c], q_recv.at[offset, c], {"kv": across(bit)}).wait_recv()
+
+    def query_forward(c):
+        held = [0]
+        for bit in bits:
+            for x in held[1:]:
+                query_copy(x, bit, c).start()
+            if bit > 1:
+                for x in held:
+                    query_wait(x ^ bit, bit, c)
+                held = held + [x ^ bit for x in held]
 
     tiles = q_w // 128
     stacked = jnp.concatenate([squeezed_wide[:, j * 128 : (j + 1) * 128] for j in range(tiles)], axis=0)
@@ -181,11 +210,8 @@
     for c in range(CHUNKS):
         for b in range(c * per, (c + 1) * per):
             qg[me, b] = qs[b].astype(BF16)
-        for o in range(n - 1, 0, -1):
-            part = qg.at[me, pl.ds(c * per, per)]
-            copy = remote(part, part, q_send.at[o, c], q_recv.at[o, c], {"kv": peer(o)})
-            copy.start()
-            started.append(copy)
+        for bit in bits:
+            query_copy(0, bit, c).start()
 
     for o in range(1, n):
         src = peer(n - o)
@@ -214,9 +240,12 @@
     l_lat.wait()
     l_rot.wait()
     for c in range(CHUNKS):
-        for o in range(1, n):
-            part = qg.at[peer(n - o), pl.ds(c * per, per)]
-            remote(part, part, q_send.at[o, c], q_recv.at[o, c], {"kv": peer(o)}).wait_recv()
+        if c == 0:
+            query_forward(0)
+        if c + 1 < CHUNKS:
+            query_forward(c + 1)
+        for offset in range(1, n, 2):
+            query_wait(offset, 1, c)
         for b in range(c * per, (c + 1) * per):
             query = jnp.concatenate([qg[j, b].astype(F32) for j in range(n)], axis=0)
             q_lat = query[:, :lat_w]

time: 47.9 us -> 46.8 us (0.977)
  Pallas kernels: 47 us -> 45.9 us
    pallas_call x1, Pallas kernels: 45.6 us -> 44.5 us  [local(): pl.pallas_call(functools.partial(kernel, (n, nt, width * n, nope_w, rope_...]
where the time goes in v3:
time: 46.8 us; the launch traced here: 46.6 us
  Pallas kernels  45.9 us (98%)
  between operations  0.64 us (1%)
    pallas_call x1, Pallas kernels, local(): pl.pallas_call(functools.partial(kernel, (n, nt, width * n, nope_w, rope_...  44.5 us
    pallas_call x1, Pallas kernels, local(): pl.pallas_call(hand_on, out_shape=tuple((jax.ShapeDtypeStruct(x.shape, x....  1.38 us

profile of v3, /device:TPU:0, one launch (start us, length us, event | category | flops | bytes accessed | tf_op | source)
XLA Modules:
  0.0 46.6 jit_solution(16924917953369752033)
XLA Ops:
  0.6 44.5 %shard_map.166 = (f32[8,512]{1,0:T(8,128)}, f32[8,1024]{1,0:T(8,128)}, f32[8,64]{1,0:T(8,128)}) custom-call(s32[8]{0:T(128)} %lens.1, bf16[8,1024]{1,0:T(8,128)(2,1)} %tok.1, f32[1,1024]{1,0:T(1,128)} %bitcast.14, f32[12,128]{1,0:T(8,128)} %bitcast.13, f32[1,1024]{1,0:T(1,128)} %bitcast.15, f32[1,512]{1,0:T(1,128)} %constant.2.clone.freq, ...), custom_call_target="tpu_custom_call" | custom-call | tf_op jit(solution)/shard_map/pallas_call | solution.py:412
  45.2 1.4 %shard_map.167 = (f32[8,512]{1,0:T(8,128)}, f32[8,1024]{1,0:T(8,128)}, f32[8,64]{1,0:T(8,128)}) custom-call(f32[8,512]{1,0:T(8,128)} %get-tuple-element.6.refs_0_, f32[8,1024]{1,0:T(8,128)} %get-tuple-element.7.refs_1_, f32[8,64]{1,0:T(8,128)} %get-tuple-element.8.refs_2_), custom_call_target="tpu_custom_call" | custom-call | tf_op jit(solution)/shard_map/pallas_call | solution.py:426
